TPU v7x, 32 devices: a whole 2x2x4 slice. The times are simulated.
32 devices in a mesh: sp: 8 (over z, y), tp: 4 (over x, core).
Axes of the slice: x: 2, y: 2, z: 4, core: 2. Of those that a mesh axis runs over, the one named last changes fastest.
Arguments:
- tokens: bfloat16 [2048, 4096], P('sp'), may hold values from -64 to 64
- norm_gain: float32 [4096], replicated, may hold values from 0.1 to 1.9
- w_query: bfloat16 [4096, 2048], P('sp', 'tp'), may hold values from -1.09375 to 1.09375
- w_key: bfloat16 [4096, 512], P('sp', 'tp'), may hold values from -0.09375 to 0.09375
- w_value: bfloat16 [4096, 512], P('sp', 'tp'), may hold values from -0.09375 to 0.09375
- w_glu: bfloat16 [4096, 2048], P('sp', 'tp'), may hold values from -0.09375 to 0.09375
- w_gate: bfloat16 [4096, 2048], P('sp', 'tp'), may hold values from -0.09375 to 0.09375
- sink_logit: float32 [32], P('tp'), may hold values from 2 to 6
- conv_taps: bfloat16 [31, 2048], P(None, 'tp'), may hold values from -12.9315817 to 12.9315817
- conv_gain: float32 [2048], P('tp'), may hold values from 0.1 to 1.9
- out_attn: bfloat16 [2048, 4096], P('sp', 'tp'), may hold values from -0.5 to 0.5
- out_conv: bfloat16 [2048, 4096], P('sp', 'tp'), may hold values from -0.125 to 0.125
Outputs:
- mixed: bfloat16 [2048, 4096], P('sp', 'tp')
All inputs are finite; a program needn't handle non-finite values.
Results may differ from a plain program's by a relative error of at most 0.008.
The roundings to bfloat16 on the way count: a program that leaves them out, or rounds other values in their place, can miss the bound.
Values may be sent and summed in bfloat16 or wider, within the bound.
A program may use at most 64 MiB of HBM per device.

v0:
```python
import math

import jax
import jax.numpy as jnp
from jax import lax
from jax.sharding import PartitionSpec as P

HEADS = 32
HEAD = 64
KV = 8
CONV = 2048
KSIZE = 31
WINDOW = 128


def passed_along(block, axis, distance):
    devices = range(lax.axis_size(axis))
    route = [(i - distance, i) for i in devices if i - distance in devices]
    return lax.ppermute(block, axis, route)


def rotate_heads(values, positions):
    half_width = values.shape[-1] // 2
    frequency = 10000.0 ** (-jnp.arange(half_width, dtype=jnp.float32) * 2.0 / values.shape[-1])
    angles = positions.astype(jnp.float32)[:, None] * frequency[None, :]
    cosine = jnp.cos(angles)[:, None, :]
    sine_part = jnp.sin(angles)[:, None, :]
    first_half = values[..., :half_width]
    second_half = values[..., half_width:]
    return jnp.concatenate(
        [
            first_half * cosine - second_half * sine_part,
            second_half * cosine + first_half * sine_part,
        ],
        axis=-1,
    )


def per_device(
    tokens,
    norm_gain,
    w_query,
    w_key,
    w_value,
    w_glu,
    w_gate,
    sink_logit,
    conv_taps,
    conv_gain,
    out_attn,
    out_conv,
):
    row_count = tokens.shape[0]
    offset_rows = lax.axis_index("sp") * row_count
    positions = offset_rows + jnp.arange(row_count, dtype=jnp.int32)
    tokens_f = tokens.astype(jnp.float32)
    normed = (
        tokens_f
        * lax.rsqrt(jnp.mean(tokens_f * tokens_f, axis=1, keepdims=True) + 1e-06)
        * norm_gain
    ).astype(jnp.bfloat16)
    local_heads = w_query.shape[1] // HEAD
    local_kv = w_key.shape[1] // HEAD
    group_size = HEADS // KV
    kv_width = local_kv * HEAD
    pieces = (
        lax.all_gather(w_query, "sp", axis=0, tiled=True),
        lax.all_gather(w_key, "sp", axis=0, tiled=True),
        lax.all_gather(w_value, "sp", axis=0, tiled=True),
        lax.all_gather(w_glu, "sp", axis=0, tiled=True),
        lax.all_gather(w_gate, "sp", axis=0, tiled=True),
    )
    query_acc, key_acc, value_acc, glu_acc, gate_acc = tuple(
        (
            jnp.dot(normed, weight_piece, preferred_element_type=jnp.float32)
            for weight_piece in pieces
        )
    )
    queries = rotate_heads(query_acc.reshape(row_count, local_heads, HEAD), positions).astype(
        jnp.bfloat16
    )
    keys_rot = rotate_heads(key_acc.reshape(row_count, local_kv, HEAD), positions).astype(
        jnp.bfloat16
    )
    keys_rot = keys_rot.reshape(row_count, kv_width)
    values_bf = value_acc.astype(jnp.bfloat16)
    kv_tail = jnp.concatenate(
        [keys_rot[row_count - WINDOW :], values_bf[row_count - WINDOW :]], axis=1
    )
    kv_rim = passed_along(kv_tail, "sp", 1)
    gated = (glu_acc * jax.nn.sigmoid(gate_acc)).astype(jnp.bfloat16)
    conv_tail = gated[row_count - (KSIZE - 1) :]
    conv_rim = passed_along(conv_tail, "sp", 1)
    block_count = row_count // WINDOW
    keys_all = jnp.concatenate([kv_rim[:, :kv_width], keys_rot], axis=0).reshape(
        block_count + 1, WINDOW, local_kv, HEAD
    )
    vals_all = jnp.concatenate([kv_rim[:, kv_width:], values_bf], axis=0).reshape(
        block_count + 1, WINDOW, local_kv, HEAD
    )
    key_blocks = jnp.concatenate([keys_all[:-1], keys_all[1:]], axis=1)
    value_blocks = jnp.concatenate([vals_all[:-1], vals_all[1:]], axis=1)
    query_block_rows = queries.reshape(block_count, WINDOW, local_kv, group_size, HEAD)
    score_matrix = jnp.einsum(
        "bqhgd,bkhd->bhgqk", query_block_rows, key_blocks, preferred_element_type=jnp.float32
    ) * (1.0 / math.sqrt(HEAD))
    block_ids = jnp.arange(block_count, dtype=jnp.int32)[:, None, None]
    query_pos = (
        offset_rows + block_ids * WINDOW + jnp.arange(WINDOW, dtype=jnp.int32)[None, :, None]
    )
    key_pos = (
        offset_rows
        + (block_ids - 1) * WINDOW
        + jnp.arange(2 * WINDOW, dtype=jnp.int32)[None, None, :]
    )
    distance = query_pos - key_pos
    allowed = (distance >= 0) & (distance < WINDOW) & (key_pos >= 0)
    score_matrix = jnp.where(allowed[:, None, None], score_matrix, -1e30)
    sink_local = sink_logit.reshape(local_kv, group_size)[None, :, :, None, None]
    highest = jnp.maximum(jnp.max(score_matrix, axis=-1, keepdims=True), sink_local)
    weights_exp = jnp.exp(score_matrix - highest)
    denom_total = jnp.sum(weights_exp, axis=-1, keepdims=True) + jnp.exp(sink_local - highest)
    weights_bfloat_half = (weights_exp / denom_total).astype(jnp.bfloat16)
    attended_values = jnp.einsum(
        "bhgqk,bkhd->bqhgd", weights_bfloat_half, value_blocks, preferred_element_type=jnp.float32
    ).astype(jnp.bfloat16)
    attended_values = attended_values.reshape(row_count, local_heads * HEAD)
    extended = jnp.concatenate([conv_rim, gated], axis=0).astype(jnp.float32)
    filtered = lax.conv_general_dilated(
        extended[None],
        conv_taps.astype(jnp.float32)[:, None, :],
        (1,),
        "VALID",
        dimension_numbers=("NWC", "WIO", "NWC"),
        feature_group_count=extended.shape[1],
        precision=lax.Precision.HIGHEST,
    )[0]
    channel_sum, channel_square = lax.psum(
        (jnp.sum(filtered, axis=1), jnp.sum(filtered * filtered, axis=1)), "tp"
    )
    mean_value = channel_sum / CONV
    variance = channel_square / CONV - mean_value * mean_value
    scaled = (filtered - mean_value[:, None]) * lax.rsqrt(variance + 1e-05)[:, None] * conv_gain
    conv_out = jax.nn.silu(scaled).astype(jnp.bfloat16)
    attn_rows, conv_rows = (
        lax.all_gather(out_attn, "sp", axis=0, tiled=True),
        lax.all_gather(out_conv, "sp", axis=0, tiled=True),
    )
    pieces = (
        lax.all_gather(attended_values, "tp", axis=1, tiled=True),
        lax.all_gather(conv_out, "tp", axis=1, tiled=True),
    )
    mixed = jnp.dot(pieces[0], attn_rows, preferred_element_type=jnp.float32) + jnp.dot(
        pieces[1], conv_rows, preferred_element_type=jnp.float32
    )
    return mixed.astype(jnp.bfloat16)


def solution(mesh):
    return jax.shard_map(
        per_device,
        mesh=mesh,
        in_specs=(
            P("sp", None),
            P(),
            P("sp", "tp"),
            P("sp", "tp"),
            P("sp", "tp"),
            P("sp", "tp"),
            P("sp", "tp"),
            P("tp"),
            P(None, "tp"),
            P("tp"),
            P("sp", "tp"),
            P("sp", "tp"),
        ),
        out_specs=P("sp", "tp"),
        check_vma=False,
    )
```

profile of v0, /device:TPU:0, one launch (start us, length us, event | category | flops | bytes accessed | tf_op | source)
XLA Modules:
  0.0 507.1 jit_solution(4216213949882157082)
XLA Ops:
  11.4 2.1 fusion
  14.0 38.5 %all-gather.12.cloned.1.call-done = bf16[4096,128]{1,0:T(8,128)(2,1)} async-done(((bf16[512,128]{1,0:T(8,128)(2,1)}), bf16[4096,128]{1,0:T(8,128)(2,1)}) %all-gather.12.cloned.1.call-update) | async-done | bytes 1048592 | tf_op jit(solution)/shard_map/all_gather | solution.py:69
  52.5 2.0 convolution_convert_fusion.1
  54.7 39.0 %all-gather.10.cloned.1.call-done = bf16[4096,128]{1,0:T(8,128)(2,1)} async-done(((bf16[512,128]{1,0:T(8,128)(2,1)}), bf16[4096,128]{1,0:T(8,128)(2,1)}) %all-gather.10.cloned.1.call-update) | async-done | bytes 1048592 | tf_op jit(solution)/shard_map/all_gather | solution.py:68
  93.7 2.2 fusion.41
  96.1 2.5 collective-permute-start
  98.7 1.8 collective-permute-done
  100.9 66.5 %all-gather.14.cloned.1.call-done = bf16[4096,512]{1,0:T(8,128)(2,1)} async-done(((bf16[512,512]{1,0:T(8,128)(2,1)}), bf16[4096,512]{1,0:T(8,128)(2,1)}) %all-gather.14.cloned.1.call-update) | async-done | bytes 4194320 | tf_op jit(solution)/shard_map/all_gather | solution.py:67
  167.4 4.0 fusion.38
  174.9 65.8 %all-gather.22.cloned.1.call-done = bf16[4096,512]{1,0:T(8,128)(2,1)} async-done(((bf16[512,512]{1,0:T(8,128)(2,1)}), bf16[4096,512]{1,0:T(8,128)(2,1)}) %all-gather.22.cloned.1.call-update) | async-done | bytes 4194320 | tf_op jit(solution)/shard_map/all_gather | solution.py:71
  240.7 3.6 fusion.7
  244.3 69.8 %all-gather.20.cloned.1.call-done = bf16[4096,512]{1,0:T(8,128)(2,1)} async-done(((bf16[512,512]{1,0:T(8,128)(2,1)}), bf16[4096,512]{1,0:T(8,128)(2,1)}) %all-gather.20.cloned.1.call-update) | async-done | bytes 4194320 | tf_op jit(solution)/shard_map/all_gather | solution.py:70
  314.0 3.5 fusion.8
  317.5 2.4 collective-permute-start.1
  320.0 1.6 collective-permute-done.1
  321.9 1.3 convolution_select_fusion
  323.9 6.1 %all-reduce = (f32[256]{0:T(256)S(1)}, f32[256]{0:T(256)S(1)}) all-reduce(f32[256]{0:T(256)S(1)} %fusion.19, f32[256]{0:T(256)S(1)} %slice_reduce_fusion), channel_id=1, replica_groups=mesh['sp'=8,'tp'=4] {'tp'}, use_global_device_ids=true, to_apply=%region_6.7 | all-reduce | flops 512 | bytes 4096 | tf_op jit(solution)/shard_map/psum | solution.py:138
  330.0 1.0 multiply_convert_fusion
  331.0 56.4 %all-gather.18.cloned.1.call-done = bf16[2048,1024]{1,0:T(8,128)(2,1)} async-done(((bf16[256,1024]{1,0:T(8,128)(2,1)}), bf16[2048,1024]{1,0:T(8,128)(2,1)}) %all-gather.18.cloned.1.call-update) | async-done | bytes 4194320 | tf_op jit(solution)/shard_map/all_gather | solution.py:146
  387.4 16.8 %all-gather.16.cloned.1.call-done = bf16[256,2048]{0,1:T(8,128)(2,1)} async-done(((bf16[256,512]{0,1:T(8,128)(2,1)}), bf16[256,2048]{0,1:T(8,128)(2,1)}) %all-gather.16.cloned.1.call-update) | async-done | bytes 1048592 | tf_op jit(solution)/shard_map/all_gather | solution.py:150
  404.2 3.8 fusion.46
  408.0 71.2 %all-gather.26.cloned.1.call-done = bf16[2048,1024]{1,0:T(8,128)(2,1)} async-done(((bf16[256,1024]{1,0:T(8,128)(2,1)}), bf16[2048,1024]{1,0:T(8,128)(2,1)}) %all-gather.26.cloned.1.call-update) | async-done | bytes 4194320 | tf_op jit(solution)/shard_map/all_gather | solution.py:147
  479.1 16.8 %all-gather.24.cloned.1.call-done = bf16[256,2048]{1,0:T(8,128)(2,1)} async-done(((bf16[256,512]{1,0:T(8,128)(2,1)}), bf16[256,2048]{1,0:T(8,128)(2,1)}) %all-gather.24.cloned.1.call-update) | async-done | bytes 1048592 | tf_op jit(solution)/shard_map/all_gather | solution.py:151
  496.0 4.6 fusion.4
  (78 shorter events, 10.5 us)
Async XLA Ops:
  6.5 315.4 %copy-start = (bf16[31,512]{1,0:T(8,128)(2,1)S(1)}, bf16[31,512]{1,0:T(8,128)(2,1)}, u32[]{:S(2)}) copy-start(bf16[31,512]{1,0:T(8,128)(2,1)} %param.20) | copy-start | bytes 95236
  6.5 46.0 %copy-start.1 = (bf16[256,4096]{1,0:T(8,128)(2,1)S(1)}, bf16[256,4096]{1,0:T(8,128)(2,1)}, u32[]{:S(2)}) copy-start(bf16[256,4096]{1,0:T(8,128)(2,1)} %param.12) | copy-start | bytes 6291460
  6.5 46.0 %copy-start.3 = (f32[4096]{0:T(1024)S(1)}, f32[4096]{0:T(1024)}, u32[]{:S(2)}) copy-start(f32[4096]{0:T(1024)} %param.13) | copy-start | bytes 49156
  6.5 46.0 %all-gather.12.cloned.1.call-start = ((), (), s32[]{:S(2)}) async-start(), calls=%async_computation.1 | async-start | bytes 1179648 | tf_op jit(solution)/shard_map/all_gather | solution.py:69
  7.3 86.4 %all-gather.10.cloned.1.call-start = ((), (), s32[]{:S(2)}) async-start(), calls=%async_computation | async-start | bytes 1179648 | tf_op jit(solution)/shard_map/all_gather | solution.py:68
  8.0 159.3 %all-gather.14.cloned.1.call-start = ((), (), s32[]{:S(2)}) async-start(), calls=%async_computation.2 | async-start | bytes 4718592 | tf_op jit(solution)/shard_map/all_gather | solution.py:67
  8.7 231.9 %all-gather.22.cloned.1.call-start = ((), (), s32[]{:S(2)}) async-start(), calls=%async_computation.6 | async-start | bytes 4718592 | tf_op jit(solution)/shard_map/all_gather | solution.py:71
  9.3 304.7 %all-gather.20.cloned.1.call-start = ((), (), s32[]{:S(2)}) async-start(), calls=%async_computation.5 | async-start | bytes 4718592 | tf_op jit(solution)/shard_map/all_gather | solution.py:70
  9.9 377.5 %all-gather.18.cloned.1.call-start = ((), (), s32[]{:S(2)}) async-start(), calls=%async_computation.4 | async-start | bytes 4718592 | tf_op jit(solution)/shard_map/all_gather | solution.py:146
  10.5 393.7 %all-gather.16.cloned.1.call-start = ((), (), s32[]{:S(2)}) async-start(), calls=%async_computation.3 | async-start | bytes 1310720 | tf_op jit(solution)/shard_map/all_gather | solution.py:150
  96.1 4.4 collective-permute-start
  174.1 305.0 %all-gather.26.cloned.1.call-start = ((), (), s32[]{:S(2)}) async-start(), calls=%async_computation.8 | async-start | bytes 4718592 | tf_op jit(solution)/shard_map/all_gather | solution.py:147
  174.9 321.1 %all-gather.24.cloned.1.call-start = ((), (), s32[]{:S(2)}) async-start(), calls=%async_computation.7 | async-start | bytes 1310720 | tf_op jit(solution)/shard_map/all_gather | solution.py:151
  244.3 77.7 %copy-start.4 = (pred[8,36]{0,1:T(8,128)(4,1)S(1)}, pred[8,36]{0,1:T(8,128)(4,1)}, u32[]{:S(2)}) copy-start(pred[8,36]{0,1:T(8,128)(4,1)} %constant.53) | copy-start | bytes 868
  317.5 4.0 collective-permute-start.1
  321.9 8.1 %copy-start.2 = (f32[512]{0:T(512)S(1)}, f32[512]{0:T(512)}, u32[]{:S(2)}) copy-start(f32[512]{0:T(512)} %param.21) | copy-start | bytes 6148
Sparse Core Ops, SparseCore 0:
  9.5 43.0 all-gather.11
  54.7 38.9 all-gather.9
  95.8 71.4 all-gather.13
  169.3 71.3 all-gather.21
  242.7 71.3 all-gather.19
  316.0 71.3 all-gather.17
  388.9 15.2 all-gather.15
  406.3 72.7 all-gather.25
  480.7 15.2 all-gather.23
where the time goes:
time: 507 us
  waiting for transfers between devices  448 us (88%)
  matrix products  26 us (5%)
  between operations  13.5 us (3%)
  blocking collectives  6.07 us (1%)
  starting transfers between devices  5.24 us (1%)
    all_gather x1, waiting for transfers between devices, per_device(): lax.all_gather(out_conv, 'sp', axis=0, tiled=True)  71.2 us
    all_gather x1, waiting for transfers between devices, per_device(): lax.all_gather(w_glu, 'sp', axis=0, tiled=True)  69.8 us
    all_gather x1, waiting for transfers between devices, per_device(): lax.all_gather(w_query, 'sp', axis=0, tiled=True)  66.5 us
    all_gather x1, waiting for transfers between devices, per_device(): lax.all_gather(w_gate, 'sp', axis=0, tiled=True)  65.8 us
    all_gather x1, waiting for transfers between devices, per_device(): lax.all_gather(out_attn, 'sp', axis=0, tiled=True)  56.4 us
    all_gather x1, waiting for transfers between devices, per_device(): lax.all_gather(w_key, 'sp', axis=0, tiled=True)  39 us
    all_gather x1, waiting for transfers between devices, per_device(): lax.all_gather(w_value, 'sp', axis=0, tiled=True)  38.5 us
    all_gather x1, waiting for transfers between devices, per_device(): lax.all_gather(conv_out, 'tp', axis=1, tiled=True)  16.8 us
  transfers between devices with their start and end apart: 11, of which 11 were waited for; matrix products, arithmetic and copies ran while one was open for 6% of the time, Pallas kernels for 0%

commit v1 on v0

--- a/solution.py
+++ b/solution.py
@@ -1,8 +1,11 @@
+import functools
 import math
 
 import jax
 import jax.numpy as jnp
 from jax import lax
+from jax.experimental import pallas as pl
+from jax.experimental.pallas import tpu as pltpu
 from jax.sharding import PartitionSpec as P
 
 HEADS = 32
@@ -34,6 +37,114 @@
         ],
         axis=-1,
     )
+
+
+def ring_gather_kernel(n, count, *refs):
+    shards, wholes = refs[:count], refs[count : 2 * count]
+    bounce = refs[2 * count : 3 * count]
+    in_sem, out_sem, send_sem, recv_sem = refs[3 * count :]
+    me = lax.axis_index("sp")
+    half = n // 2
+    odd = lax.rem(me, 2)
+    place = (1 - odd) * lax.div(me, 2) + odd * (n - 1 - lax.div(me, 2))
+
+    def device_at(position):
+        spot = lax.rem(position + 2 * n, n)
+        back = lax.div(spot, half)
+        return (1 - back) * 2 * spot + back * (2 * (n - 1 - spot) + 1)
+
+    ahead, behind = device_at(place + 1), device_at(place - 1)
+    barrier = pltpu.get_barrier_semaphore()
+    for neighbour in (ahead, behind):
+        pl.semaphore_signal(
+            barrier, inc=1, device_id={"sp": neighbour}, device_id_type=pl.DeviceIdType.MESH
+        )
+    pl.semaphore_wait(barrier, 2)
+
+    def block(array, owner, way):
+        rows = shards[array].shape[0]
+        part = rows // 2
+        start = pl.multiple_of(owner * rows + way * part, part)
+        return wholes[array].at[pl.ds(start, part)]
+
+    def hop(array, step, way):
+        owner = device_at(place - step) if way == 0 else device_at(place + step)
+        part = shards[array].shape[0] // 2
+        target = block(array, owner, way)
+        source = shards[array].at[pl.ds(way * part, part)] if step == 0 else target
+        return pltpu.make_async_remote_copy(
+            src_ref=source,
+            dst_ref=target,
+            send_sem=send_sem.at[way, step, array],
+            recv_sem=recv_sem.at[way, step, array],
+            device_id={"sp": ahead if way == 0 else behind},
+            device_id_type=pl.DeviceIdType.MESH,
+        )
+
+    def arrival(array, step, way):
+        owner = device_at(place - step - 1) if way == 0 else device_at(place + step + 1)
+        target = block(array, owner, way)
+        return pltpu.make_async_remote_copy(
+            src_ref=target,
+            dst_ref=target,
+            send_sem=send_sem.at[way, step, array],
+            recv_sem=recv_sem.at[way, step, array],
+            device_id={"sp": ahead if way == 0 else behind},
+            device_id_type=pl.DeviceIdType.MESH,
+        )
+
+    for array in range(count):
+        for way in range(2):
+            hop(array, 0, way).start()
+    loads = [
+        pltpu.make_async_copy(shards[a], bounce[a], in_sem.at[a]) for a in range(count)
+    ]
+    for load in loads:
+        load.start()
+    stores = []
+    for a in range(count):
+        loads[a].wait()
+        rows = shards[a].shape[0]
+        mine = wholes[a].at[pl.ds(pl.multiple_of(me * rows, rows), rows)]
+        stores.append(pltpu.make_async_copy(bounce[a], mine, out_sem.at[a]))
+        stores[a].start()
+    for step in range(1, n - 1):
+        for array in range(count):
+            for way in range(2):
+                arrival(array, step - 1, way).wait_recv()
+                hop(array, step, way).start()
+    for array in range(count):
+        for way in range(2):
+            arrival(array, n - 2, way).wait_recv()
+    for step in range(n - 1):
+        for array in range(count):
+            for way in range(2):
+                hop(array, step, way).wait_send()
+    for store in stores:
+        store.wait()
+
+
+def ring_gather(arrays, collective_id):
+    n = lax.axis_size("sp")
+    count = len(arrays)
+    return pl.pallas_call(
+        functools.partial(ring_gather_kernel, n, count),
+        out_shape=[
+            jax.ShapeDtypeStruct((n * a.shape[0],) + a.shape[1:], a.dtype) for a in arrays
+        ],
+        in_specs=[pl.BlockSpec(memory_space=pl.ANY)] * count,
+        out_specs=[pl.BlockSpec(memory_space=pl.ANY)] * count,
+        scratch_shapes=[pltpu.VMEM(a.shape, a.dtype) for a in arrays]
+        + [
+            pltpu.SemaphoreType.DMA((count,)),
+            pltpu.SemaphoreType.DMA((count,)),
+            pltpu.SemaphoreType.DMA((2, n - 1, count)),
+            pltpu.SemaphoreType.DMA((2, n - 1, count)),
+        ],
+        compiler_params=pltpu.CompilerParams(
+            collective_id=collective_id, has_side_effects=True
+        ),
+    )(*arrays)
 
 
 def per_device(
@@ -63,12 +174,8 @@
     local_kv = w_key.shape[1] // HEAD
     group_size = HEADS // KV
     kv_width = local_kv * HEAD
-    pieces = (
-        lax.all_gather(w_query, "sp", axis=0, tiled=True),
-        lax.all_gather(w_key, "sp", axis=0, tiled=True),
-        lax.all_gather(w_value, "sp", axis=0, tiled=True),
-        lax.all_gather(w_glu, "sp", axis=0, tiled=True),
-        lax.all_gather(w_gate, "sp", axis=0, tiled=True),
+    *pieces, attn_rows, conv_rows = ring_gather(
+        (w_query, w_key, w_value, w_glu, w_gate, out_attn, out_conv), 0
     )
     query_acc, key_acc, value_acc, glu_acc, gate_acc = tuple(
         (
@@ -142,10 +249,6 @@
     variance = channel_square / CONV - mean_value * mean_value
     scaled = (filtered - mean_value[:, None]) * lax.rsqrt(variance + 1e-05)[:, None] * conv_gain
     conv_out = jax.nn.silu(scaled).astype(jnp.bfloat16)
-    attn_rows, conv_rows = (
-        lax.all_gather(out_attn, "sp", axis=0, tiled=True),
-        lax.all_gather(out_conv, "sp", axis=0, tiled=True),
-    )
     pieces = (
         lax.all_gather(attended_values, "tp", axis=1, tiled=True),
         lax.all_gather(conv_out, "tp", axis=1, tiled=True),

time: 507 us -> 299 us (0.59)
  waiting for transfers between devices: 448 us -> 15.6 us
  Pallas kernels: 0 us -> 224 us
    all_gather x7 -> x0, waiting for transfers between devices: 407 us -> none  [the longest x1 71.2 us: per_device(): lax.all_gather(out_conv, 'sp', axis=0, tiled=True)]
    pallas_call x0 -> x1, Pallas kernels: none -> 224 us  [ring_gather(): pl.pallas_call(functools.partial(ring_gather_kernel, n, count), out_shape...]
    all_gather x1, waiting for transfers between devices: 16.8 us -> 0.02 us  [per_device(): lax.all_gather(attended_values, 'tp', axis=1, tiled=True)]
  transfers between devices with their start and end apart: 11 -> 4, of which waited for: 11 -> 2; matrix products, arithmetic and copies ran while one was open for 6% -> 7% of each run, Pallas kernels for 0% -> 0%
where the time goes in v1:
time: 299 us
  Pallas kernels  224 us (75%)
  matrix products  25.7 us (9%)
  waiting for transfers between devices  15.6 us (5%)
  between operations  13.8 us (5%)
  starting transfers between devices  7.09 us (2%)
  blocking collectives  5.67 us (2%)
  other arithmetic  4.76 us (2%)
    pallas_call x1, Pallas kernels, ring_gather(): pl.pallas_call(functools.partial(ring_gather_kernel, n, count), out_shape...  224 us
    dot_general x5, matrix products, per_device(): jnp.dot(normed, weight_piece, preferred_element_type=jnp.float32)  15 us
    all_gather x1, waiting for transfers between devices, per_device(): lax.all_gather(conv_out, 'tp', axis=1, tiled=True)  14.1 us
    ppermute x2, starting transfers between devices, passed_along(): return lax.ppermute(block, axis, route)  7.05 us
  transfers between devices with their start and end apart: 4, of which 2 were waited for; matrix products, arithmetic and copies ran while one was open for 7% of the time, Pallas kernels for 0%

profile of v1, /device:TPU:0, one launch (start us, length us, event | category | flops | bytes accessed | tf_op | source)
XLA Modules:
  0.0 298.9 jit_solution(12133648533888614277)
XLA Ops:
  6.6 2.2 fusion
  8.8 223.7 %shard_map.118 = (bf16[4096,512]{1,0:T(8,128)(2,1)}, bf16[4096,128]{1,0:T(8,128)(2,1)}, bf16[4096,128]{1,0:T(8,128)(2,1)}, bf16[4096,512]{1,0:T(8,128)(2,1)}, bf...) custom-call(bf16[512,512]{1,0:T(8,128)(2,1)} %refs_0_.1, ...), custom_call_target="tpu_custom_call" | custom-call | tf_op jit(solution)/shard_map/pallas_call | solution.py:130
  232.6 2.3 fusion.41
  234.9 0.8 convolution_convert_fusion.1
  235.7 0.2 multiply_cosine_fusion
  236.1 3.4 %collective-permute-start = (bf16[128,256]{1,0:T(8,128)(2,1)S(1)}, bf16[128,256]{1,0:T(8,128)(2,1)S(1)}, u32[]{:S(2)}, u32[]{:S(2)}) collective-permute-start(bf16[128,256]{1,0:T(8,128)(2,1)S(1)} %pad_maximum_fusion.2), channel_id=1, source_target_pairs={{0,4},{4,8},{8,12},{12,16},{16,20},{20,24},{24,28},{1,5},{5,9},{9,... | collective-permute-start | bytes 196616 | tf_op jit(solution)/shard_map/ppermute | solution.py:22
  240.1 4.1 %fusion.38 = f32[256,512]{0,1:T(8,128)S(1)} fusion(bf16[4096,512]{1,0:T(8,128)(2,1)} %get-tuple-element.14, bf16[256,4096]{1,0:T(8,128)(2,1)S(1)} %copy-done.1, f32[4096]{0:T(1024)S(1)} %copy-done.4, f32[256]{0:T(256)S(1)} %add_rsqrt_fusion.1), kind=kOutput, calls=%fused_computation.80 | convolution fusion | flops 1077936128 | bytes 6833152 | tf_op jit(solution)/shard_map/dot_general | solution.py:182
  244.4 4.3 %fusion.7 = f32[256,512]{1,0:T(8,128)} fusion(bf16[4096,512]{1,0:T(8,128)(2,1)} %get-tuple-element.17, bf16[256,4096]{1,0:T(8,128)(2,1)S(1)} %copy-done.1, f32[4096]{0:T(1024)S(1)} %copy-done.4, f32[256]{0:T(256)S(1)} %add_rsqrt_fusion.1), kind=kOutput, calls=%fused_computation.15 | convolution fusion | flops 1078329344 | bytes 6833152 | tf_op jit(solution)/shard_map/dot_general | solution.py:182
  248.7 0.2 fusion.25
  249.4 0.5 fusion.44
  250.0 0.3 fusion.3
  250.4 0.5 fusion.9
  250.9 0.3 copy.36
  251.2 0.7 copy.55
  252.0 3.5 %fusion.8 = bf16[256,512]{1,0:T(8,128)(2,1)S(1)} fusion(f32[256,512]{1,0:T(8,128)S(1)} %copy-done.7, bf16[4096,512]{1,0:T(8,128)(2,1)} %get-tuple-element.16, bf16[256,4096]{1,0:T(8,128)(2,1)S(1)} %copy-done.1, f32[4096]{0:T(1024)S(1)} %copy-done.4, f32[256]{0:T(256)S(1)} %add_rsqrt_fusion.1), kind=kOutput, calls=%fused_computation.16 | convolution fusion | flops 1078198272 | bytes 7095296 | tf_op jit(solution)/shard_map/dot_general | solution.py:182
  255.5 3.6 %collective-permute-start.1 = (bf16[30,512]{1,0:T(8,128)(2,1)S(1)}, bf16[30,512]{1,0:T(8,128)(2,1)S(1)}, u32[]{:S(2)}, u32[]{:S(2)}) collective-permute-start(bf16[30,512]{1,0:T(8,128)(2,1)S(1)} %slice.73), channel_id=1, source_target_pairs={{0,4},{4,8},{8,12},{12,16},{16,20},{20,24},{24,28},{1,5},{5,9},{9,... | collective-permute-start | bytes 92168 | tf_op jit(solution)/shard_map/ppermute | solution.py:22
  259.1 1.4 collective-permute-done.1
  260.9 1.4 convolution_select_fusion
  262.3 0.3 copy.40
  262.9 5.7 %all-reduce = (f32[256]{0:T(256)S(1)}, f32[256]{0:T(256)S(1)}) all-reduce(f32[256]{0:T(256)S(1)} %fusion.19, f32[256]{0:T(256)S(1)} %slice_reduce_fusion), channel_id=1, replica_groups=mesh['sp'=8,'tp'=4] {'tp'}, use_global_device_ids=true, to_apply=%region_6.7 | all-reduce | flops 512 | bytes 4096 | tf_op jit(solution)/shard_map/psum | solution.py:245
  268.6 1.0 multiply_convert_fusion
  269.6 3.8 %fusion.46 = f32[256,1024]{1,0:T(8,128)S(1)} fusion(bf16[256,2048]{0,1:T(8,128)(2,1)} %all-gather.3.cloned.1.call-done, bf16[2048,1024]{1,0:T(8,128)(2,1)} %get-tuple-element.15), kind=kOutput, calls=%fused_computation.85 | convolution fusion | flops 1073741824 | bytes 6291456 | tf_op jit(solution)/shard_map/dot_general | solution.py:256
  273.4 14.1 %all-gather.5.cloned.1.call-done = bf16[256,2048]{1,0:T(8,128)(2,1)} async-done(((bf16[256,512]{1,0:T(8,128)(2,1)}), bf16[256,2048]{1,0:T(8,128)(2,1)}) %all-gather.5.cloned.1.call-update) | async-done | bytes 1048592 | tf_op jit(solution)/shard_map/all_gather | solution.py:254
  287.5 4.6 %fusion.4 = bf16[256,1024]{1,0:T(8,128)(2,1)} fusion(f32[256,1024]{1,0:T(8,128)S(1)} %fusion.46, bf16[256,2048]{1,0:T(8,128)(2,1)} %all-gather.5.cloned.1.call-done, bf16[2048,1024]{1,0:T(8,128)(2,1)} %get-tuple-element.18), kind=kOutput, calls=%fused_computation.10 | convolution fusion | flops 1074266112 | bytes 6815744 | tf_op jit(solution)/shard_map/dot_general | solution.py:256
  (64 shorter events, 2.2 us)
Async XLA Ops:
  6.5 254.3 %copy-start = (bf16[31,512]{1,0:T(8,128)(2,1)S(1)}, bf16[31,512]{1,0:T(8,128)(2,1)}, u32[]{:S(2)}) copy-start(bf16[31,512]{1,0:T(8,128)(2,1)} %param.20) | copy-start | bytes 95236
  6.5 226.0 %copy-start.1 = (bf16[256,4096]{1,0:T(8,128)(2,1)S(1)}, bf16[256,4096]{1,0:T(8,128)(2,1)}, u32[]{:S(2)}) copy-start(bf16[256,4096]{1,0:T(8,128)(2,1)} %param.12) | copy-start | bytes 6291460
  6.5 226.0 %copy-start.4 = (f32[4096]{0:T(1024)S(1)}, f32[4096]{0:T(1024)}, u32[]{:S(2)}) copy-start(f32[4096]{0:T(1024)} %param.13) | copy-start | bytes 49156
  6.5 263.0 %all-gather.3.cloned.1.call-start = ((), (), s32[]{:S(2)}) async-start(), calls=%async_computation | async-start | bytes 1310720 | tf_op jit(solution)/shard_map/all_gather | solution.py:253
  232.5 2.3 copy-start.3
  232.6 7.2 %copy-start.5 = (f32[8]{0:T(128)S(1)}, f32[8]{0:T(128)}, u32[]{:S(2)}) copy-start(f32[8]{0:T(128)} %param.19) | copy-start | bytes 100
  236.1 12.8 %collective-permute-start = (bf16[128,256]{1,0:T(8,128)(2,1)S(1)}, bf16[128,256]{1,0:T(8,128)(2,1)S(1)}, u32[]{:S(2)}, u32[]{:S(2)}) collective-permute-start(bf16[128,256]{1,0:T(8,128)(2,1)S(1)} %pad_maximum_fusion.2), channel_id=1, source_target_pairs={{0,4},{4,8},{8,12},{12,16},{16,20},{20,24},{24,28},{1,5},{5,9},{9,... | collective-permute-start | bytes 196616 | tf_op jit(solution)/shard_map/ppermute | solution.py:22
  250.4 1.6 copy-start.7
  251.9 35.6 %all-gather.5.cloned.1.call-start = ((), (), s32[]{:S(2)}) async-start(), calls=%async_computation.1 | async-start | bytes 1310720 | tf_op jit(solution)/shard_map/all_gather | solution.py:254
  252.0 8.9 %copy-start.6 = (pred[8,36]{0,1:T(8,128)(4,1)S(1)}, pred[8,36]{0,1:T(8,128)(4,1)}, u32[]{:S(2)}) copy-start(pred[8,36]{0,1:T(8,128)(4,1)} %constant.53) | copy-start | bytes 868
  255.5 5.0 %collective-permute-start.1 = (bf16[30,512]{1,0:T(8,128)(2,1)S(1)}, bf16[30,512]{1,0:T(8,128)(2,1)S(1)}, u32[]{:S(2)}, u32[]{:S(2)}) collective-permute-start(bf16[30,512]{1,0:T(8,128)(2,1)S(1)} %slice.73), channel_id=1, source_target_pairs={{0,4},{4,8},{8,12},{12,16},{16,20},{20,24},{24,28},{1,5},{5,9},{9,... | collective-permute-start | bytes 92168 | tf_op jit(solution)/shard_map/ppermute | solution.py:22
  260.9 7.7 %copy-start.2 = (f32[512]{0:T(512)S(1)}, f32[512]{0:T(512)}, u32[]{:S(2)}) copy-start(f32[512]{0:T(512)} %param.21) | copy-start | bytes 6148
Sparse Core Ops, SparseCore 0:
  252.0 15.8 all-gather.2
  269.7 17.7 all-gather.4
